TPU v7x, 32 devices: a whole 2x2x4 slice. The times are simulated.
32 devices in a mesh: sp: 8 (over z, x), tp: 4 (over y, core).
Axes of the slice: x: 2, y: 2, z: 4, core: 2. Of those that a mesh axis runs over, the one named last changes fastest.
Arguments:
- stream_in: bfloat16 [2048, 2048], P(('sp', 'tp')), may hold values from -6 to 6
- pre_gate: bfloat16 [2048, 1024], P('sp', 'tp'), may hold values from -6 to 6
- value_in: bfloat16 [2048, 1024], P('sp', 'tp'), may hold values from -6 to 6
- post_gate: bfloat16 [2048, 1024], P('sp', 'tp'), may hold values from -6 to 6
- conv_taps: bfloat16 [3, 1024], P(None, 'tp'), may hold values from -3 to 3
- out_weight: bfloat16 [1024, 2048], P('tp'), may hold values from -0.1875 to 0.1875
- route_ids: int32 [2048, 4], P('sp'), may hold values from 0 to 7, all different within a row; in each aligned block of 64 rows (0 to 63, 64 to 127, ...) at most 64 rows name the same one
- route_weight: float32 [2048, 4], P('sp'), may hold values from 0.1 to 1
- ffn_gain: bfloat16 [2048], replicated, may hold values from 0.099609375 to 1.8984375
- post_gain: bfloat16 [2048], replicated, may hold values from 0.099609375 to 1.8984375
- gate_proj: bfloat16 [8, 2048, 2048], P('sp', None, 'tp'), may hold values from -0.39648438 to 0.39648438
- up_proj: bfloat16 [8, 2048, 2048], P('sp', None, 'tp'), may hold values from -0.39648438 to 0.39648438
- down_proj: bfloat16 [8, 2048, 2048], P('sp', None, 'tp'), may hold values from -0.125 to 0.125
Outputs:
- layer_out: bfloat16 [2048, 2048], P(('sp', 'tp'))
Inputs may be any that keep to these rules, and one draw needn't show every extreme that they name: `route_ids`: in each aligned block of 64 positions, a row names 4 different experts and no expert is named by more than 64 rows; in every draw some expert reaches 64 in some block.
All inputs are finite; a program needn't handle non-finite values.
Results may differ from a plain program's by a relative error of at most 0.014.
Values may be sent and summed in bfloat16 or wider, within the bound.
A program may use at most 64 MiB of HBM per device.

v0:
```python
import jax
import jax.numpy as jnp
from jax import lax
from jax.sharding import PartitionSpec as P

clamp_limit = 7.0
sigmoid_scale = 1.702
epsilon = 1e-06


def passed_along(array, axis, by):
    count = lax.axis_size(axis)
    pairs = [(i, i + by) for i in range(count) if 0 <= i + by < count]
    return lax.ppermute(array, axis, pairs)


def clamped_units(gate_pre, up_pre):
    gate_cut = jnp.minimum(gate_pre, clamp_limit)
    up_cut = jnp.clip(up_pre, -clamp_limit, clamp_limit)
    return (up_cut + 1.0) * (gate_cut * jax.nn.sigmoid(sigmoid_scale * gate_cut))


def scaled_norm(values, gain):
    return (
        values
        * lax.rsqrt(jnp.mean(values * values, axis=-1, keepdims=True) + epsilon)
        * gain.astype(jnp.float32)
    )


def block_ranks(route_rows, experts, block_rows):
    flattened = route_rows.reshape(-1)
    entries = flattened.shape[0]
    span_width = block_rows * route_rows.shape[1]
    onehot = (flattened[:, None] == jnp.arange(experts, dtype=jnp.int32)[None, :]).astype(jnp.int32)
    blocked = onehot.reshape(entries // span_width, span_width, experts)
    before = jnp.cumsum(blocked, axis=1) - blocked
    return jnp.sum(before * blocked, axis=2).reshape(route_rows.shape)


def slot_picker(slot_index, table_size):
    matches = slot_index[None, :, :] == jnp.arange(table_size, dtype=jnp.int32)[:, None, None]
    return jnp.any(matches, axis=2).astype(jnp.bfloat16)


def local(
    stream_in,
    pre_gate,
    value_in,
    post_gate,
    conv_taps,
    out_weight,
    route_ids,
    route_weight,
    ffn_gain,
    post_gain,
    gate_proj,
    up_proj,
    down_proj,
):
    sp_count = lax.axis_size("sp")
    tp_count = lax.axis_size("tp")
    seq_rows = pre_gate.shape[0]
    own_rows = seq_rows // tp_count
    top_count = route_ids.shape[1]
    slots_each = 2 * own_rows * top_count // sp_count
    tap_count = conv_taps.shape[0]
    gated_input = (pre_gate.astype(jnp.float32) * value_in.astype(jnp.float32)).astype(jnp.bfloat16)
    rim_rows = passed_along(gated_input[seq_rows - tap_count + 1 :], "sp", 1)
    padded = jnp.concatenate([rim_rows, gated_input], 0).astype(jnp.float32)
    convolved = jnp.zeros(gated_input.shape, jnp.float32)
    for tap_index in range(tap_count):
        convolved = (
            convolved
            + conv_taps[tap_index].astype(jnp.float32)[None, :]
            * padded[tap_index : tap_index + seq_rows]
        )
    mixer_out = (post_gate.astype(jnp.float32) * convolved).astype(jnp.bfloat16)
    weight_rows = mixer_out
    projected = lax.psum_scatter(
        jnp.dot(weight_rows, out_weight, preferred_element_type=jnp.float32),
        "tp",
        scatter_dimension=0,
        tiled=True,
    )
    residual = (stream_in.astype(jnp.float32) + projected).astype(jnp.bfloat16)
    normed = scaled_norm(residual.astype(jnp.float32), ffn_gain).astype(jnp.bfloat16)
    slot_rank = block_ranks(route_ids, sp_count, own_rows)
    block_of = (jnp.arange(seq_rows, dtype=jnp.int32) // own_rows)[:, None]
    tp_index = lax.axis_index("tp")
    own_ids = lax.dynamic_slice_in_dim(route_ids, tp_index * own_rows, own_rows, 0)
    own_rank = lax.dynamic_slice_in_dim(slot_rank, tp_index * own_rows, own_rows, 0)
    own_slot = own_ids * slots_each + own_rank
    picker = slot_picker(own_slot, sp_count * slots_each)
    outgoing = jnp.dot(picker, normed, preferred_element_type=jnp.float32).astype(jnp.bfloat16)
    arrived = lax.all_to_all(outgoing, "sp", split_axis=0, concat_axis=0, tiled=True)
    portion = lax.all_gather(arrived, "tp", axis=0, tiled=True)
    gate_pre = jnp.dot(portion, gate_proj[0], preferred_element_type=jnp.float32)
    up_pre = jnp.dot(portion, up_proj[0], preferred_element_type=jnp.float32)
    hidden = clamped_units(gate_pre, up_pre).astype(jnp.bfloat16)
    weight_rows = down_proj[0]
    column_out = jnp.dot(
        lax.all_gather(hidden, "tp", axis=1, tiled=True),
        weight_rows,
        preferred_element_type=jnp.float32,
    ).astype(jnp.bfloat16)
    column_width = column_out.shape[1]
    returned = lax.all_to_all(
        column_out.reshape(tp_count, sp_count, slots_each, column_width),
        "sp",
        split_axis=1,
        concat_axis=1,
        tiled=True,
    )
    home_index = (block_of * sp_count + route_ids) * slots_each + slot_rank
    gathered_out = jnp.take(returned.reshape(-1, column_width), home_index.reshape(-1), axis=0)
    gathered_out = gathered_out.astype(jnp.float32).reshape(seq_rows, top_count, column_width)
    combined_cols = jnp.sum(gathered_out * route_weight[:, :, None], axis=1).astype(jnp.bfloat16)
    combined = lax.all_to_all(combined_cols, "tp", split_axis=0, concat_axis=1, tiled=True)
    layer_out = residual.astype(jnp.float32) + scaled_norm(combined.astype(jnp.float32), post_gain)
    return layer_out.astype(jnp.bfloat16)


def solution(mesh):
    placed = (
        P(("sp", "tp"), None),
        P("sp", "tp"),
        P("sp", "tp"),
        P("sp", "tp"),
        P(None, "tp"),
        P("tp", None),
        P("sp", None),
        P("sp", None),
        P(),
        P(),
        P("sp", None, "tp"),
        P("sp", None, "tp"),
        P("sp", None, "tp"),
    )
    return jax.shard_map(
        local, mesh=mesh, in_specs=placed, out_specs=P(("sp", "tp"), None), check_vma=False
    )
```

profile of v0, /device:TPU:0, one launch (start us, length us, event | category | flops | bytes accessed | tf_op | source)
XLA Modules:
  0.0 330.7 jit_solution(6274343751186609560)
XLA Ops:
  6.6 1.2 multiply_convert_fusion.1
  7.8 4.9 %collective-permute-start = (bf16[2,256]{1,0:T(2,128)(2,1)S(1)}, bf16[2,256]{1,0:T(2,128)(2,1)S(1)}, u32[]{:S(2)}, u32[]{:S(2)}) collective-permute-start(bf16[2,256]{1,0:T(2,128)(2,1)S(1)} %slice.38), channel_id=1, source_target_pairs={{0,4},{4,8},{8,12},{12,16},{16,20},{20,24},{24,28},{1,5},{5,9},{9,... | collective-permute-start | bytes 3080 | tf_op jit(solution)/shard_map/ppermute | solution.py:14
  12.6 0.8 slice_convert_fusion.2
  13.4 0.5 collective-permute-done
  13.9 3.1 fusion.17
  17.2 0.1 copy.54
  17.6 2.3 reduce-window.6
  20.2 0.1 reshape.118
  20.5 0.1 fusion.9
  20.6 29.9 %reduce-scatter.2.cloned.1.call-done = f32[64,2048]{1,0:T(8,128)} async-done(((f32[256,2048]{1,0:T(8,128)}), f32[64,2048]{1,0:T(8,128)}) %reduce-scatter.2.cloned.1.call-update) | async-done | bytes 524304 | tf_op jit(solution)/shard_map/reduce_scatter | solution.py:80
  50.5 1.2 fusion.5
  51.7 0.8 convolution_convert_fusion.1
  52.5 53.5 %all_to_all.27 = bf16[8,64,2048]{2,1,0:T(8,128)(2,1)} all-to-all(bf16[8,64,2048]{2,1,0:T(8,128)(2,1)S(1)} %bitcast.40), channel_id=1, replica_groups=mesh['sp'=8,'tp'=4] {'sp'}, dimensions={0} | all-to-all | bytes 4194304 | tf_op jit(solution)/shard_map/all_to_all | solution.py:96
  106.1 56.5 %all-gather.3.cloned.1.call-done = bf16[2048,2048]{1,0:T(8,128)(2,1)} async-done(((bf16[512,2048]{1,0:T(8,128)(2,1)}), bf16[2048,2048]{1,0:T(8,128)(2,1)}) %all-gather.3.cloned.1.call-update) | async-done | bytes 8388624 | tf_op jit(solution)/shard_map/all_gather | solution.py:97
  162.5 7.7 %fusion.2 = f32[2048,512]{1,0:T(8,128)S(1)} fusion(bf16[2048,2048]{1,0:T(8,128)(2,1)} %all-gather.3.cloned.1.call-done, bf16[1,2048,512]{2,1,0:T(8,128)(2,1)S(1)} %copy-done), kind=kOutput, calls=%fused_computation.6 | convolution fusion | flops 4294967296 | bytes 14680064 | tf_op jit(solution)/shard_map/dot_general | solution.py:99
  170.2 6.7 %multiply_convert_fusion = bf16[2048,512]{1,0:T(8,128)(2,1)} fusion(f32[2048,512]{1,0:T(8,128)S(1)} %fusion.2, bf16[2048,2048]{1,0:T(8,128)(2,1)S(1)} %copy-done.6, bf16[1,2048,512]{2,1,0:T(8,128)(2,1)S(1)} %copy-done.7), kind=kOutput, calls=%fused_computation.1 | convolution fusion | flops 4305453056 | bytes 16777216 | tf_op jit(solution)/shard_map/dot_general | solution.py:98
  177.0 58.4 %all-gather.5.cloned.1.call-done = bf16[2048,2048]{1,0:T(8,128)(2,1)} async-done(((bf16[2048,512]{1,0:T(8,128)(2,1)}), bf16[2048,2048]{1,0:T(8,128)(2,1)}) %all-gather.5.cloned.1.call-update) | async-done | bytes 8388624 | tf_op jit(solution)/shard_map/all_gather | solution.py:103
  235.4 8.5 %convolution_convert_fusion = bf16[2048,512]{1,0:T(8,128)(2,1)S(1)} fusion(bf16[2048,2048]{1,0:T(8,128)(2,1)} %all-gather.5.cloned.1.call-done, bf16[1,2048,512]{2,1,0:T(8,128)(2,1)} %param.25), kind=kOutput, calls=%fused_computation.2 | convolution fusion | flops 4296015872 | bytes 12582912 | tf_op jit(solution)/shard_map/dot_general | solution.py:102
  243.9 1.4 copy.61
  245.3 5.5 %all-to-all-start.1 = ((bf16[4,8,64,512]{3,2,0,1:T(8,128)(2,1)}), bf16[4,8,64,512]{3,2,0,1:T(8,128)(2,1)}, u32[]{:S(2)}, u32[]{:S(2)}) async-start(bf16[4,8,64,512]{3,2,0,1:T(8,128)(2,1)} %copy.61), calls=%async_computation.2 | async-start | bytes 4194304 | tf_op jit(solution)/shard_map/all_to_all | solution.py:108
  250.9 0.1 copy.63
  251.1 0.8 copy.59
  251.9 0.1 copy.64
  252.1 47.5 %all-to-all-done.1 = bf16[4,8,64,512]{3,2,0,1:T(8,128)(2,1)} async-done(((bf16[4,8,64,512]{3,2,0,1:T(8,128)(2,1)}), bf16[4,8,64,512]{3,2,0,1:T(8,128)(2,1)}, u32[]{:S(2)}, u32[]{:S(2)}) %all-to-all-start.1) | async-done | bytes 2097184 | tf_op jit(solution)/shard_map/all_to_all | solution.py:108
  299.6 3.1 copy.62
  302.7 5.9 %gather_fusion = bf16[1024,512]{1,0:T(8,128)(2,1)S(1)} fusion(bf16[2048,512]{1,0:T(8,128)(2,1)} %bitcast.38, s32[1024]{0:T(1024)S(1)} %broadcast_clamp_fusion), kind=kCustom, calls=%fused_computation | custom fusion | bytes 2101248 | tf_op jit(solution)/shard_map/jit(_take)/gather | solution.py:116
  308.6 1.1 gather.7
  309.7 4.0 %multiply_reduce_fusion = bf16[256,512]{1,0:T(8,128)(2,1)} fusion(f32[256,4]{1,0:T(8,128)S(1)} %copy.64, bf16[256,4,512]{2,1,0:T(4,128)(2,1)} %gather.7, pred[256,4]{1,0:T(8,128)(4,1)} %copy.59), kind=kLoop, calls=%fused_computation.8 | loop fusion | flops 1966080 | bytes 1315840 | tf_op jit(solution)/shard_map/reduce_sum | solution.py:118
  313.7 3.4 %all-to-all-start.2 = ((bf16[4,64,512]{2,1,0:T(8,128)(2,1)}), bf16[4,64,512]{2,1,0:T(8,128)(2,1)S(1)}, u32[]{:S(2)}, u32[]{:S(2)}) async-start(bf16[4,64,512]{2,1,0:T(8,128)(2,1)} %bitcast.14), calls=%async_computation.3 | async-start | bytes 524288 | tf_op jit(solution)/shard_map/all_to_all | solution.py:119
  317.1 6.0 %all-to-all-done.2 = bf16[4,64,512]{2,1,0:T(8,128)(2,1)S(1)} async-done(((bf16[4,64,512]{2,1,0:T(8,128)(2,1)}), bf16[4,64,512]{2,1,0:T(8,128)(2,1)S(1)}, u32[]{:S(2)}, u32[]{:S(2)}) %all-to-all-start.2) | async-done | bytes 262176 | tf_op jit(solution)/shard_map/all_to_all | solution.py:119
  323.2 0.2 fusion.4
  323.3 0.9 fusion.8
  (46 shorter events, 1.2 us)
Async XLA Ops:
  6.5 156.0 %copy-start = (bf16[1,2048,512]{2,1,0:T(8,128)(2,1)S(1)}, bf16[1,2048,512]{2,1,0:T(8,128)(2,1)}, u32[]{:S(2)}) copy-start(bf16[1,2048,512]{2,1,0:T(8,128)(2,1)} %param.24) | copy-start | bytes 6291460
  6.5 10.6 %copy-start.2 = (s32[256,4]{0,1:T(4,128)S(1)}, s32[256,4]{0,1:T(4,128)}, u32[]{:S(2)}) copy-start(s32[256,4]{0,1:T(4,128)} %param.19) | copy-start | bytes 12292
  6.5 13.8 %copy-start.3 = (bf16[2048]{0:T(1024)(128)(2,1)S(1)}, bf16[2048]{0:T(1024)(128)(2,1)}, u32[]{:S(2)}) copy-start(bf16[2048]{0:T(1024)(128)(2,1)} %param.21) | copy-start | bytes 12292
  6.5 43.9 %copy-start.1 = (bf16[64,2048]{1,0:T(8,128)(2,1)S(1)}, bf16[64,2048]{1,0:T(8,128)(2,1)}, u32[]{:S(2)}) copy-start(bf16[64,2048]{1,0:T(8,128)(2,1)} %param.13) | copy-start | bytes 786436
  6.5 43.9 %reduce-scatter.2.cloned.1.call-start = ((), (), s32[]{:S(2)}) async-start(), calls=%async_computation.4 | async-start | bytes 2621440 | tf_op jit(solution)/shard_map/reduce_scatter | solution.py:80
  7.8 6.2 %collective-permute-start = (bf16[2,256]{1,0:T(2,128)(2,1)S(1)}, bf16[2,256]{1,0:T(2,128)(2,1)S(1)}, u32[]{:S(2)}, u32[]{:S(2)}) collective-permute-start(bf16[2,256]{1,0:T(2,128)(2,1)S(1)} %slice.38), channel_id=1, source_target_pairs={{0,4},{4,8},{8,12},{12,16},{16,20},{20,24},{24,28},{1,5},{5,9},{9,... | collective-permute-start | bytes 3080 | tf_op jit(solution)/shard_map/ppermute | solution.py:14
  17.1 145.4 %all-gather.3.cloned.1.call-start = ((), (), s32[]{:S(2)}) async-start(), calls=%async_computation.5 | async-start | bytes 10485760 | tf_op jit(solution)/shard_map/all_gather | solution.py:97
  106.0 129.3 %all-gather.5.cloned.1.call-start = ((), (), s32[]{:S(2)}) async-start(), calls=%async_computation.6 | async-start | bytes 10485760 | tf_op jit(solution)/shard_map/all_gather | solution.py:103
  162.5 7.7 %copy-start.6 = (bf16[2048,2048]{1,0:T(8,128)(2,1)S(1)}, bf16[2048,2048]{1,0:T(8,128)(2,1)}, u32[]{:S(2)}) copy-start(bf16[2048,2048]{1,0:T(8,128)(2,1)} %all-gather.3.cloned.1.call-done) | copy-start | bytes 25165828
  162.5 7.7 %copy-start.7 = (bf16[1,2048,512]{2,1,0:T(8,128)(2,1)S(1)}, bf16[1,2048,512]{2,1,0:T(8,128)(2,1)}, u32[]{:S(2)}) copy-start(bf16[1,2048,512]{2,1,0:T(8,128)(2,1)} %param.23) | copy-start | bytes 6291460
  243.9 8.0 %copy-start.4 = (f32[256,4]{0,1:T(4,128)S(1)}, f32[256,4]{0,1:T(4,128)}, u32[]{:S(2)}) copy-start(f32[256,4]{0,1:T(4,128)} %param.20) | copy-start | bytes 12292
  245.3 54.3 %all-to-all-start.1 = ((bf16[4,8,64,512]{3,2,0,1:T(8,128)(2,1)}), bf16[4,8,64,512]{3,2,0,1:T(8,128)(2,1)}, u32[]{:S(2)}, u32[]{:S(2)}) async-start(bf16[4,8,64,512]{3,2,0,1:T(8,128)(2,1)} %copy.61), calls=%async_computation.2 | async-start | bytes 4194304 | tf_op jit(solution)/shard_map/all_to_all | solution.py:108
  302.7 14.4 %copy-start.5 = (bf16[2048]{0:T(1024)(128)(2,1)S(1)}, bf16[2048]{0:T(1024)(128)(2,1)}, u32[]{:S(2)}) copy-start(bf16[2048]{0:T(1024)(128)(2,1)} %param.22) | copy-start | bytes 12292
  313.7 9.4 %all-to-all-start.2 = ((bf16[4,64,512]{2,1,0:T(8,128)(2,1)}), bf16[4,64,512]{2,1,0:T(8,128)(2,1)S(1)}, u32[]{:S(2)}, u32[]{:S(2)}) async-start(bf16[4,64,512]{2,1,0:T(8,128)(2,1)} %bitcast.14), calls=%async_computation.3 | async-start | bytes 524288 | tf_op jit(solution)/shard_map/all_to_all | solution.py:119
Sparse Core Ops, SparseCore 0:
  17.2 33.2 reduce-scatter.1
  106.1 56.3 all-gather.2
  177.1 58.2 all-gather.4
where the time goes:
time: 331 us
  waiting for transfers between devices  199 us (60%)
  blocking collectives  53.5 us (16%)
  matrix products  26.8 us (8%)
  starting transfers between devices  13.9 us (4%)
  local copies, waits for them, and re-layouts  13.6 us (4%)
  between operations  13.3 us (4%)
  other arithmetic  10.9 us (3%)
    all_gather x1, waiting for transfers between devices, local(): lax.all_gather(hidden, 'tp', axis=1, tiled=True)  58.4 us
    all_gather x1, waiting for transfers between devices, local(): portion = lax.all_gather(arrived, 'tp', axis=0, tiled=True)  56.5 us
    all_to_all x1, blocking collectives, local(): lax.all_to_all(outgoing, 'sp', split_axis=0, concat_axis=0, tiled=True)  53.5 us
    all_to_all x1, waiting for transfers between devices, local(): lax.all_to_all(column_out.reshape(tp_count, sp_count, slots_each, column_...  47.5 us
    reduce_scatter x1, waiting for transfers between devices, local(): lax.psum_scatter(jnp.dot(weight_rows, out_weight, preferred_element_type=...  29.9 us
    dot_general x1, matrix products, local(): jnp.dot(lax.all_gather(hidden, 'tp', axis=1, tiled=True), weight_rows, pr...  8.49 us
    dot_general x1, matrix products, local(): up_pre = jnp.dot(portion, up_proj[0], preferred_element_type=jnp.float32)  7.66 us
    gather x2, local copies, waits for them, and re-layouts, local(): jnp.take(returned.reshape(-1, column_width), home_index.reshape(-1), axis=0)  6.98 us
  transfers between devices with their start and end apart: 6, of which 6 were waited for; matrix products, arithmetic and copies ran while one was open for 2% of the time, Pallas kernels for 0%

commit v1 on v0

--- a/solution.py
+++ b/solution.py
@@ -6,6 +6,17 @@
 clamp_limit = 7.0
 sigmoid_scale = 1.702
 epsilon = 1e-06
+
+
+def turned_line(array, mesh_axis, along):
+    peers = lax.axis_size(mesh_axis)
+    right = [(i, (i + 1) % peers) for i in range(peers)]
+    parts = [array]
+    for far in range(1, peers):
+        parts = [lax.ppermute(parts[0], mesh_axis, right), *parts]
+    out = jnp.concatenate(parts, axis=along)
+    shift = (lax.axis_index(mesh_axis) + 1) * parts[-1].shape[along]
+    return jnp.roll(out, shift, axis=along)
 
 
 def passed_along(array, axis, by):
@@ -94,7 +105,7 @@
     picker = slot_picker(own_slot, sp_count * slots_each)
     outgoing = jnp.dot(picker, normed, preferred_element_type=jnp.float32).astype(jnp.bfloat16)
     arrived = lax.all_to_all(outgoing, "sp", split_axis=0, concat_axis=0, tiled=True)
-    portion = lax.all_gather(arrived, "tp", axis=0, tiled=True)
+    portion = turned_line(arrived, "tp", 0)
     gate_pre = jnp.dot(portion, gate_proj[0], preferred_element_type=jnp.float32)
     up_pre = jnp.dot(portion, up_proj[0], preferred_element_type=jnp.float32)
     hidden = clamped_units(gate_pre, up_pre).astype(jnp.bfloat16)

time: 331 us -> 358 us (1.082)
  waiting for transfers between devices: 199 us -> 217 us
  local copies, waits for them, and re-layouts: 13.6 us -> 24.3 us
    ppermute x0 -> x3, waiting for transfers between devices: none -> 76.8 us  [turned_line(): parts = [lax.ppermute(parts[0], mesh_axis, right), *parts]]
    all_gather x1 -> x0, waiting for transfers between devices: 56.5 us -> none  [local(): portion = lax.all_gather(arrived, 'tp', axis=0, tiled=True)]
    unnamed x18 -> x31, local copies, waits for them, and re-layouts: 0.3 us -> 10.9 us
  transfers between devices with their start and end apart: 6 -> 8, of which waited for: 6 -> 8; matrix products, arithmetic and copies ran while one was open for 2% -> 2% of each run, Pallas kernels for 0% -> 0%
where the time goes in v1:
time: 358 us; the launch traced here: 357 us
  waiting for transfers between devices  217 us (61%)
  blocking collectives  53.4 us (15%)
  local copies, waits for them, and re-layouts  24.3 us (7%)
  matrix products  23.6 us (7%)
  starting transfers between devices  13.9 us (4%)
  between operations  13.7 us (4%)
  other arithmetic  10.9 us (3%)
    ppermute x3, waiting for transfers between devices, turned_line(): parts = [lax.ppermute(parts[0], mesh_axis, right), *parts]  76.8 us
    all_gather x1, waiting for transfers between devices, local(): lax.all_gather(hidden, 'tp', axis=1, tiled=True)  56.5 us
    all_to_all x1, blocking collectives, local(): lax.all_to_all(outgoing, 'sp', split_axis=0, concat_axis=0, tiled=True)  53.4 us
    all_to_all x1, waiting for transfers between devices, local(): lax.all_to_all(column_out.reshape(tp_count, sp_count, slots_each, column_...  47.5 us
    reduce_scatter x1, waiting for transfers between devices, local(): lax.psum_scatter(jnp.dot(weight_rows, out_weight, preferred_element_type=...  29.8 us
    unnamed x31, local copies, waits for them, and re-layouts  10.9 us
    dot_general x1, matrix products, local(): jnp.dot(lax.all_gather(hidden, 'tp', axis=1, tiled=True), weight_rows, pr...  8.49 us
  transfers between devices with their start and end apart: 8, of which 8 were waited for; matrix products, arithmetic and copies ran while one was open for 2% of the time, Pallas kernels for 0%

profile of v1, /device:TPU:0, one launch (start us, length us, event | category | flops | bytes accessed | tf_op | source)
XLA Modules:
  0.0 356.9 jit_solution(15303656589087495576)
XLA Ops:
  6.6 1.2 multiply_convert_fusion.1
  7.8 4.9 %collective-permute-start = (bf16[2,256]{1,0:T(2,128)(2,1)S(1)}, bf16[2,256]{1,0:T(2,128)(2,1)S(1)}, u32[]{:S(2)}, u32[]{:S(2)}) collective-permute-start(bf16[2,256]{1,0:T(2,128)(2,1)S(1)} %slice.38), channel_id=1, source_target_pairs={{0,4},{4,8},{8,12},{12,16},{16,20},{20,24},{24,28},{1,5},{5,9},{9,... | collective-permute-start | bytes 3080 | tf_op jit(solution)/shard_map/ppermute | solution.py:25
  12.6 0.8 slice_convert_fusion.2
  13.9 3.1 fusion.22
  17.6 2.3 reduce-window.6
  20.6 29.8 %reduce-scatter.2.cloned.1.call-done = f32[64,2048]{1,0:T(8,128)} async-done(((f32[256,2048]{1,0:T(8,128)}), f32[64,2048]{1,0:T(8,128)}) %reduce-scatter.2.cloned.1.call-update) | async-done | bytes 524304 | tf_op jit(solution)/shard_map/reduce_scatter | solution.py:91
  50.5 1.2 fusion.10
  51.7 0.8 convolution_convert_fusion.1
  52.5 53.4 %all_to_all.27 = bf16[8,64,2048]{2,1,0:T(8,128)(2,1)S(1)} all-to-all(bf16[8,64,2048]{2,1,0:T(8,128)(2,1)S(1)} %bitcast.40), channel_id=1, replica_groups=mesh['sp'=8,'tp'=4] {'sp'}, dimensions={0} | all-to-all | bytes 4194304 | tf_op jit(solution)/shard_map/all_to_all | solution.py:107
  105.9 1.3 copy-done.1
  107.2 25.5 %collective-permute-done.1 = bf16[512,2048]{1,0:T(8,128)(2,1)S(1)} collective-permute-done((bf16[512,2048]{1,0:T(8,128)(2,1)S(1)}, bf16[512,2048]{1,0:T(8,128)(2,1)S(1)}, u32[]{:S(2)}, u32[]{:S(2)}) %collective-permute-start.1) | collective-permute-done | bytes 2097184 | tf_op jit(solution)/shard_map/ppermute | solution.py:16
  132.7 1.3 copy-done.3
  134.0 25.6 %collective-permute-done.2 = bf16[512,2048]{1,0:T(8,128)(2,1)} collective-permute-done((bf16[512,2048]{1,0:T(8,128)(2,1)S(1)}, bf16[512,2048]{1,0:T(8,128)(2,1)}, u32[]{:S(2)}, u32[]{:S(2)}) %collective-permute-start.2) | collective-permute-done | bytes 2097184 | tf_op jit(solution)/shard_map/ppermute | solution.py:16
  159.6 25.8 %collective-permute-done.3 = bf16[512,2048]{1,0:T(8,128)(2,1)} collective-permute-done((bf16[512,2048]{1,0:T(8,128)(2,1)}, bf16[512,2048]{1,0:T(8,128)(2,1)}, u32[]{:S(2)}, u32[]{:S(2)}) %collective-permute-start.3) | collective-permute-done | bytes 2097184 | tf_op jit(solution)/shard_map/ppermute | solution.py:16
  185.3 1.8 constant_dynamic-update-slice_fusion.7
  187.2 2.0 constant_dynamic-update-slice_fusion.6
  189.5 1.8 constant_dynamic-update-slice_fusion.3
  191.4 1.8 constant_dynamic-update-slice_fusion.2
  193.5 4.5 %fusion.2 = f32[2048,512]{1,0:T(8,128)S(1)} fusion(bf16[4096,2048]{1,0:T(8,128)(2,1)S(1)} %constant_dynamic-update-slice_fusion, s32[]{:T(128)S(6)} %select_n.52, bf16[1,2048,512]{2,1,0:T(8,128)(2,1)S(1)} %copy-done), kind=kOutput, calls=%fused_computation.3 | convolution fusion | flops 4294967296 | bytes 14680068 | tf_op jit(solution)/shard_map/dot_general | solution.py:110
  198.1 6.7 %multiply_convert_fusion = bf16[2048,512]{1,0:T(8,128)(2,1)} fusion(f32[2048,512]{1,0:T(8,128)S(1)} %fusion.2, bf16[4096,2048]{1,0:T(8,128)(2,1)S(1)} %constant_dynamic-update-slice_fusion, s32[]{:T(128)S(6)} %select_n.52, bf16[1,2048,512]{2,1,0:T(8,128)(2,1)S(1)} %copy-done.10), kind=kOutput, calls=%fused_computation.5 | convolution fusion | flops 4305453056 | bytes 16777220 | tf_op jit(solution)/shard_map/dot_general | solution.py:109
  204.7 56.5 %all-gather.2.cloned.1.call-done = bf16[2048,2048]{1,0:T(8,128)(2,1)} async-done(((bf16[2048,512]{1,0:T(8,128)(2,1)}), bf16[2048,2048]{1,0:T(8,128)(2,1)}) %all-gather.2.cloned.1.call-update) | async-done | bytes 8388624 | tf_op jit(solution)/shard_map/all_gather | solution.py:114
  261.3 8.5 %convolution_convert_fusion = bf16[2048,512]{1,0:T(8,128)(2,1)S(1)} fusion(bf16[2048,2048]{1,0:T(8,128)(2,1)} %all-gather.2.cloned.1.call-done, bf16[1,2048,512]{2,1,0:T(8,128)(2,1)} %param.25), kind=kOutput, calls=%fused_computation.6 | convolution fusion | flops 4296015872 | bytes 12582912 | tf_op jit(solution)/shard_map/dot_general | solution.py:113
  269.8 1.4 copy.61
  271.2 5.5 %all-to-all-start.1 = ((bf16[4,8,64,512]{3,2,0,1:T(8,128)(2,1)}), bf16[4,8,64,512]{3,2,0,1:T(8,128)(2,1)}, u32[]{:S(2)}, u32[]{:S(2)}) async-start(bf16[4,8,64,512]{3,2,0,1:T(8,128)(2,1)} %copy.61), calls=%async_computation.2 | async-start | bytes 4194304 | tf_op jit(solution)/shard_map/all_to_all | solution.py:119
  278.0 47.5 %all-to-all-done.1 = bf16[4,8,64,512]{3,2,0,1:T(8,128)(2,1)} async-done(((bf16[4,8,64,512]{3,2,0,1:T(8,128)(2,1)}), bf16[4,8,64,512]{3,2,0,1:T(8,128)(2,1)}, u32[]{:S(2)}, u32[]{:S(2)}) %all-to-all-start.1) | async-done | bytes 2097184 | tf_op jit(solution)/shard_map/all_to_all | solution.py:119
  325.5 3.1 copy.62
  328.6 5.9 %gather_fusion = bf16[1024,512]{1,0:T(8,128)(2,1)S(1)} fusion(bf16[2048,512]{1,0:T(8,128)(2,1)} %bitcast.36, s32[1024]{0:T(1024)S(1)} %broadcast_clamp_fusion), kind=kCustom, calls=%fused_computation | custom fusion | bytes 2101248 | tf_op jit(solution)/shard_map/jit(_take)/gather | solution.py:127
  334.5 1.1 gather.7
  335.6 4.0 %multiply_reduce_fusion = bf16[256,512]{1,0:T(8,128)(2,1)} fusion(f32[256,4]{1,0:T(8,128)S(1)} %copy.64, bf16[256,4,512]{2,1,0:T(4,128)(2,1)} %gather.7, pred[256,4]{1,0:T(8,128)(4,1)} %copy.59), kind=kLoop, calls=%fused_computation.11 | loop fusion | flops 1966080 | bytes 1315840 | tf_op jit(solution)/shard_map/reduce_sum | solution.py:129
  339.6 3.4 all-to-all-start.2
  343.0 6.0 %all-to-all-done.2 = bf16[4,64,512]{2,1,0:T(8,128)(2,1)S(1)} async-done(((bf16[4,64,512]{2,1,0:T(8,128)(2,1)}), bf16[4,64,512]{2,1,0:T(8,128)(2,1)S(1)}, u32[]{:S(2)}, u32[]{:S(2)}) %all-to-all-start.2) | async-done | bytes 262176 | tf_op jit(solution)/shard_map/all_to_all | solution.py:130
  349.2 0.9 fusion.13
  (63 shorter events, 3.9 us)
Async XLA Ops:
  6.5 187.0 %copy-start = (bf16[1,2048,512]{2,1,0:T(8,128)(2,1)S(1)}, bf16[1,2048,512]{2,1,0:T(8,128)(2,1)}, u32[]{:S(2)}) copy-start(bf16[1,2048,512]{2,1,0:T(8,128)(2,1)} %param.24) | copy-start | bytes 6291460
  6.5 10.6 %copy-start.6 = (s32[256,4]{0,1:T(4,128)S(1)}, s32[256,4]{0,1:T(4,128)}, u32[]{:S(2)}) copy-start(s32[256,4]{0,1:T(4,128)} %param.19) | copy-start | bytes 12292
  6.5 13.8 %copy-start.7 = (bf16[2048]{0:T(1024)(128)(2,1)S(1)}, bf16[2048]{0:T(1024)(128)(2,1)}, u32[]{:S(2)}) copy-start(bf16[2048]{0:T(1024)(128)(2,1)} %param.21) | copy-start | bytes 12292
  6.5 43.9 %copy-start.5 = (bf16[64,2048]{1,0:T(8,128)(2,1)S(1)}, bf16[64,2048]{1,0:T(8,128)(2,1)}, u32[]{:S(2)}) copy-start(bf16[64,2048]{1,0:T(8,128)(2,1)} %param.13) | copy-start | bytes 786436
  6.5 43.9 %reduce-scatter.2.cloned.1.call-start = ((), (), s32[]{:S(2)}) async-start(), calls=%async_computation.4 | async-start | bytes 2621440 | tf_op jit(solution)/shard_map/reduce_scatter | solution.py:91
  7.8 6.2 %collective-permute-start = (bf16[2,256]{1,0:T(2,128)(2,1)S(1)}, bf16[2,256]{1,0:T(2,128)(2,1)S(1)}, u32[]{:S(2)}, u32[]{:S(2)}) collective-permute-start(bf16[2,256]{1,0:T(2,128)(2,1)S(1)} %slice.38), channel_id=1, source_target_pairs={{0,4},{4,8},{8,12},{12,16},{16,20},{20,24},{24,28},{1,5},{5,9},{9,... | collective-permute-start | bytes 3080 | tf_op jit(solution)/shard_map/ppermute | solution.py:25
  17.1 244.2 %all-gather.2.cloned.1.call-start = ((), (), s32[]{:S(2)}) async-start(), calls=%async_computation.5 | async-start | bytes 10485760 | tf_op jit(solution)/shard_map/all_gather | solution.py:114
  105.9 1.3 copy-start.1
  107.2 25.5 %collective-permute-start.1 = (bf16[512,2048]{1,0:T(8,128)(2,1)S(1)}, bf16[512,2048]{1,0:T(8,128)(2,1)S(1)}, u32[]{:S(2)}, u32[]{:S(2)}) collective-permute-start(bf16[512,2048]{1,0:T(8,128)(2,1)S(1)} %bitcast.37), channel_id=1, source_target_pairs={{0,1},{1,2},{2,3},{3,0},{4,5},{5,6},{6,7},{7,4},{8,9},{9,10},{10,1... | collective-permute-start | bytes 6291464 | tf_op jit(solution)/shard_map/ppermute | solution.py:16
  132.7 1.3 copy-start.3
  134.0 25.6 %collective-permute-start.2 = (bf16[512,2048]{1,0:T(8,128)(2,1)S(1)}, bf16[512,2048]{1,0:T(8,128)(2,1)}, u32[]{:S(2)}, u32[]{:S(2)}) collective-permute-start(bf16[512,2048]{1,0:T(8,128)(2,1)S(1)} %collective-permute-done.1), channel_id=1, source_target_pairs={{0,1},{1,2},{2,3},{3,0},{4,5},{5,6},{6,7},{7,4},{8,9},{9,10},{10,1... | collective-permute-start | bytes 6291464 | tf_op jit(solution)/shard_map/ppermute | solution.py:16
  159.6 25.8 %collective-permute-start.3 = (bf16[512,2048]{1,0:T(8,128)(2,1)}, bf16[512,2048]{1,0:T(8,128)(2,1)}, u32[]{:S(2)}, u32[]{:S(2)}) collective-permute-start(bf16[512,2048]{1,0:T(8,128)(2,1)} %collective-permute-done.2), channel_id=1, source_target_pairs={{0,1},{1,2},{2,3},{3,0},{4,5},{5,6},{6,7},{7,4},{8,9},{9,10},{10,1... | collective-permute-start | bytes 6291464 | tf_op jit(solution)/shard_map/ppermute | solution.py:16
  159.6 29.6 %copy-start.4 = (bf16[512,2048]{1,0:T(8,128)(2,1)S(1)}, bf16[512,2048]{1,0:T(8,128)(2,1)}, u32[]{:S(2)}) copy-start(bf16[512,2048]{1,0:T(8,128)(2,1)} %copy-done.3) | copy-start | bytes 6291460
  187.2 2.2 copy-start.2
  193.5 4.5 %copy-start.10 = (bf16[1,2048,512]{2,1,0:T(8,128)(2,1)S(1)}, bf16[1,2048,512]{2,1,0:T(8,128)(2,1)}, u32[]{:S(2)}) copy-start(bf16[1,2048,512]{2,1,0:T(8,128)(2,1)} %param.23) | copy-start | bytes 6291460
  269.8 8.0 %copy-start.8 = (f32[256,4]{0,1:T(4,128)S(1)}, f32[256,4]{0,1:T(4,128)}, u32[]{:S(2)}) copy-start(f32[256,4]{0,1:T(4,128)} %param.20) | copy-start | bytes 12292
  271.2 54.3 %all-to-all-start.1 = ((bf16[4,8,64,512]{3,2,0,1:T(8,128)(2,1)}), bf16[4,8,64,512]{3,2,0,1:T(8,128)(2,1)}, u32[]{:S(2)}, u32[]{:S(2)}) async-start(bf16[4,8,64,512]{3,2,0,1:T(8,128)(2,1)} %copy.61), calls=%async_computation.2 | async-start | bytes 4194304 | tf_op jit(solution)/shard_map/all_to_all | solution.py:119
  328.6 14.4 %copy-start.9 = (bf16[2048]{0:T(1024)(128)(2,1)S(1)}, bf16[2048]{0:T(1024)(128)(2,1)}, u32[]{:S(2)}) copy-start(bf16[2048]{0:T(1024)(128)(2,1)} %param.22) | copy-start | bytes 12292
  339.6 9.4 %all-to-all-start.2 = ((bf16[4,64,512]{2,1,0:T(8,128)(2,1)}), bf16[4,64,512]{2,1,0:T(8,128)(2,1)S(1)}, u32[]{:S(2)}, u32[]{:S(2)}) async-start(bf16[4,64,512]{2,1,0:T(8,128)(2,1)} %bitcast.14), calls=%async_computation.3 | async-start | bytes 524288 | tf_op jit(solution)/shard_map/all_to_all | solution.py:130
Sparse Core Ops, SparseCore 0:
  17.2 33.2 reduce-scatter.1
  204.9 56.3 all-gather.1
